TPU v7x, 32 devices: a whole 2x2x4 slice. The times are simulated.
32 devices in a mesh: grp: 2 (over y), ep: 8 (over z, x), tp: 2 (over core).
Axes of the slice: x: 2, y: 2, z: 4, core: 2. Of those that a mesh axis runs over, the one named last changes fastest.
Arguments:
- tokens: bfloat16 [4096, 2048], P(('grp', 'ep'), 'tp'), parts along dimension 0, may hold values from -6 to 6
- norm_gain: bfloat16 [2048], P('tp'), may hold values from 0.099609375 to 1.8984375
- w_gate: bfloat16 [8, 2048, 1024], P('ep', None, 'tp'), may hold values from -0.125 to 0.125
- w_up: bfloat16 [8, 2048, 1024], P('ep', None, 'tp'), may hold values from -0.125 to 0.125
- w_down: bfloat16 [8, 1024, 2048], P('ep', 'tp'), may hold values from -0.1875 to 0.1875
- expert_ids: int32 [4096, 2], P(('grp', 'ep')), parts along dimension 0, may hold values from 0 to 7, as said below
- combine: float32 [4096, 2], P(('grp', 'ep')), parts along dimension 0, may hold values from 0.1 to 1
- final_gain: bfloat16 [2048], P('tp'), may hold values from 0.099609375 to 1.8984375
Outputs:
- result: bfloat16 [4096, 2048], P(('grp', 'ep'), 'tp'), parts along dimension 0
There are 2 independent parts, one for each index of `grp`. A program takes and returns all parts, laid end to end along the dimension named above; an argument that names none is the same for every part. Nothing has to cross between parts.
Inputs may be any that keep to these rules, and one draw needn't show every extreme that they name: `expert_ids`: the experts form 4 groups of consecutive ids of equal size; the 2 experts of a row are different and lie in one group. Among the rows of one index of ep no expert is named more than 160 times, and in each such block some expert is named exactly 160 times.
All inputs are finite; a program needn't handle non-finite values.
Results may differ from a plain program's by a relative error of at most 0.0077.
Values may be sent and summed in bfloat16 or wider, within the bound.
A program may use at most 64 MiB of HBM per device.

v0:
```python
import functools

import jax
import jax.numpy as jnp
from jax import lax
from jax.experimental import pallas as pl
from jax.experimental.pallas import tpu as pltpu
from jax.sharding import PartitionSpec as P

GROUPS = 4
EPS = 1e-06
LEAD = 1
MESH = pl.DeviceIdType.MESH
bf16, f32 = jnp.bfloat16, jnp.float32


def general(tokens, norm_gain, w_gate, w_up, w_down, expert_ids, combine, final_gain):
    eps = EPS
    tok_dev, half = tokens.shape
    n_ep = lax.axis_size("ep")
    n_tp = lax.axis_size("tp")
    width = half * n_tp
    exp_dev = w_gate.shape[0]
    experts = exp_dev * n_ep
    per_group = experts // GROUPS
    capacity = tok_dev // 8 * 5 * 2 // per_group
    top = expert_ids.shape[1]
    narrow = tokens.astype(jnp.float32)
    squares = lax.psum(jnp.sum(narrow * narrow, axis=1), "tp")
    scale = lax.rsqrt(squares[:, None] / width + eps)
    normed = (narrow * scale * norm_gain.astype(jnp.float32)).astype(jnp.bfloat16)
    columns = normed.shape[1]
    flat = expert_ids.reshape(-1)
    onehot = (flat[:, None] == jnp.arange(experts, dtype=jnp.int32)[None, :]).astype(jnp.int32)
    ranking = jnp.sum(jnp.cumsum(onehot, axis=0) * onehot, axis=1) - 1
    target = flat * capacity + ranking
    sources = jnp.arange(tok_dev * top, dtype=jnp.int32) // top
    owner = jnp.full((experts * capacity,), tok_dev, jnp.int32).at[target].set(sources)
    padded = jnp.concatenate([normed, jnp.zeros((1, columns), jnp.bfloat16)], axis=0)
    outgoing = padded[owner].reshape(n_ep, exp_dev * capacity, columns)
    arrived = lax.all_to_all(outgoing, "ep", split_axis=0, concat_axis=0, tiled=True)
    rows = (
        arrived.reshape(n_ep, exp_dev, capacity, columns)
        .transpose(1, 0, 2, 3)
        .reshape(exp_dev, n_ep * capacity, columns)
    )
    piece = lax.all_gather(rows, "tp", axis=2, tiled=True)
    gate = jnp.einsum("erd,edf->erf", piece, w_gate, preferred_element_type=jnp.float32)
    upper = jnp.einsum("erd,edf->erf", piece, w_up, preferred_element_type=jnp.float32)
    hidden = (jax.nn.silu(gate) * upper).astype(jnp.bfloat16)
    partial_out = jnp.einsum(
        "erf,efd->erd", hidden, w_down, preferred_element_type=jnp.float32
    ).astype(jnp.bfloat16)
    shares = (
        lax.psum_scatter(partial_out, "tp", scatter_dimension=2, tiled=True)
        .astype(jnp.float32)
        .astype(jnp.bfloat16)
    )
    homeward = (
        shares.reshape(exp_dev, n_ep, capacity, half)
        .transpose(1, 0, 2, 3)
        .reshape(n_ep, exp_dev * capacity, half)
    )
    returned = lax.all_to_all(homeward, "ep", split_axis=0, concat_axis=0, tiled=True).reshape(
        experts * capacity, half
    )
    picked = returned[target].astype(jnp.float32).reshape(tok_dev, top, half)
    mixed = jnp.sum(picked * combine[:, :, None], axis=1)
    totals = lax.psum(jnp.sum(mixed * mixed, axis=1), "tp")
    norm = lax.rsqrt(totals[:, None] / width + eps)
    return (mixed * norm * final_gain.astype(jnp.float32)).astype(jnp.bfloat16)


def fold(v):
    v = v * v
    out = v[:, :128]
    for i in range(1, v.shape[1] // 128):
        out = out + v[:, i * 128 : (i + 1) * 128]
    return out


def paired_kernel(
    G, cap, tok_ref, gain_ref, ids_ref, comb_ref, wg_hbm, wu_hbm, wd_hbm, out_ref,
    wg, wu, wd, xbuf, sbuf, meta, psend, pown, precv, ebuf, xret, zbuf, ret, sq,
    wsem, sq_s, sq_r, z_s, z_r, m_s, m_r, x_s, x_r, t_s, t_r, p_s, p_r, e_s, e_r, h_s, h_r,
):
    rows, half = tok_ref.shape
    ep, c = lax.axis_index("ep"), lax.axis_index("tp")
    g, j = ep // 2, ep % 2
    other = {"ep": g * 2 + (1 - j)}
    core = {"tp": 1 - c}

    cut = cap // 2

    def flip(a, d):
        return (a % 2 + d % 2) % 2 + 2 * ((a // 2 + d // 2) % 2)

    def plane(d):
        return {"ep": flip(g, d) * 2 + j}

    inner = ((g + 1) // 2) % 2
    order = [0, 1, 2 + inner, 3 - inner]

    barrier = pltpu.get_barrier_semaphore()
    for dev in [core, other] + [plane(d) for d in range(1, G)]:
        pl.semaphore_signal(barrier, inc=1, device_id=dev, device_id_type=MESH)

    loads = []
    for i, h in enumerate((c, 1 - c)):
        at = pl.ds(pl.multiple_of(h * half, half), half)
        loads.append(pltpu.make_async_copy(wg_hbm.at[0, at, :], wg.at[i], wsem.at[i]))
        loads.append(pltpu.make_async_copy(wu_hbm.at[0, at, :], wu.at[i], wsem.at[2 + i]))
        loads.append(pltpu.make_async_copy(wd_hbm.at[0, :, at], wd.at[i], wsem.at[4 + i]))
    for load in loads:
        load.start()

    sent = []

    def send(src, dst, s, r, dev):
        copy = pltpu.make_async_remote_copy(
            src_ref=src, dst_ref=dst, send_sem=s, recv_sem=r, device_id=dev, device_id_type=MESH
        )
        copy.start()
        sent.append(copy)
        return copy

    x = tok_ref[...].astype(f32)
    sq[0] = fold(x)

    group = ids_ref[0:1, :] // 2
    slot8 = lax.broadcasted_iota(jnp.int32, (8, rows), 0)
    onehot = (slot8 == group).astype(f32)
    up_to = lax.broadcasted_iota(jnp.int32, (rows, rows), 0) <= lax.broadcasted_iota(
        jnp.int32, (rows, rows), 1
    )
    counted = jnp.dot(onehot.astype(bf16), up_to.astype(f32).astype(bf16), preferred_element_type=f32)
    rank = jnp.sum(onehot * counted, axis=0, keepdims=True) - 1.0
    offset = flip(group, g)
    target = offset * cap + rank.astype(jnp.int32)
    first = ids_ref[0:1, :] % 2 == 0
    c0, c1 = comb_ref[0:1, :], comb_ref[1:2, :]
    table = jnp.where(slot8 == 0, jnp.where(first, c0, c1), 0.0)
    table = jnp.where(slot8 == 1, jnp.where(first, c1, c0), table)
    table = jnp.where(slot8 == 2, rank, table)
    table = jnp.where(slot8 == 3, group.astype(f32), table)
    meta[0] = table
    pick = (lax.broadcasted_iota(jnp.int32, (G * cap, rows), 0) == target).astype(f32).astype(bf16)

    pl.semaphore_wait(barrier, 1 + G)
    first_sq = send(sq.at[0], sq.at[1], sq_s.at[0], sq_r.at[0], core)
    metas = [None] + [
        send(meta.at[0], meta.at[d], m_s.at[d], m_r.at[d], plane(d)) for d in order[1:]
    ]
    first_sq.wait_recv()
    total = jnp.sum(sq[0] + sq[1], axis=1, keepdims=True)
    scale = lax.rsqrt(total / (2 * half) + EPS)
    normed = (x * scale * gain_ref[...].astype(f32)[None, :]).astype(bf16)

    def gather(d):
        return jnp.dot(
            pick[d * cap : (d + 1) * cap], normed, preferred_element_type=f32
        ).astype(bf16)

    units = [(d, r) for d in order for r in range(2)]
    U = len(units)
    zs, xs, ts, fs, ps, es, hs = ([None] * U for _ in range(7))

    def arrived(u):
        d, r = units[u]
        if zs[u] is not None:
            zs[u].wait_recv()
        mine = xbuf.at[0, d, r, 0]
        xs[u] = send(mine, xbuf.at[0, d, r, 1], x_s.at[d, r], x_r.at[d, r], other)
        ts[u] = send(mine, xbuf.at[1, d, r, 0], t_s.at[d, r, 0], t_r.at[d, r, 0], core)

    def crossed(u):
        d, r = units[u]
        xs[u].wait_recv()
        fs[u] = send(
            xbuf.at[0, d, r, 1], xbuf.at[1, d, r, 1], t_s.at[d, r, 1], t_r.at[d, r, 1], core
        )

    def compute(u):
        d, r = units[u]
        ts[u].wait_recv()
        fs[u].wait_recv()
        a = xbuf[0, d, r].reshape(2 * cut, half)
        b = xbuf[1, d, r].reshape(2 * cut, half)
        gate = jnp.dot(a, wg[0], preferred_element_type=f32) + jnp.dot(
            b, wg[1], preferred_element_type=f32
        )
        upper = jnp.dot(a, wu[0], preferred_element_type=f32) + jnp.dot(
            b, wu[1], preferred_element_type=f32
        )
        hidden = (gate / (1.0 + jnp.exp(-gate)) * upper).astype(bf16)
        away = jnp.dot(hidden, wd[1], preferred_element_type=f32)
        psend[d, r] = away.astype(bf16).reshape(2, cut, half)
        ps[u] = send(psend.at[d, r], precv.at[d, r], p_s.at[d, r], p_r.at[d, r], core)
        home = jnp.dot(hidden, wd[0], preferred_element_type=f32)
        pown[d, r] = home.astype(bf16).reshape(2, cut, half)

    def summed(u):
        d, r = units[u]
        ps[u].wait_recv()
        ebuf[d, r, 1] = (pown[d, r, 1].astype(f32) + precv[d, r, 1].astype(f32)).astype(bf16)
        es[u] = send(ebuf.at[d, r, 1], xret.at[d, r], e_s.at[d, r], e_r.at[d, r], other)
        ebuf[d, r, 0] = (pown[d, r, 0].astype(f32) + precv[d, r, 0].astype(f32)).astype(bf16)

    def mix(u):
        d, r = units[u]
        if u >= 2 and r == 0:
            metas[u // 2].wait_recv()
        tab = meta[d]
        slots = lax.broadcasted_iota(jnp.int32, (cut, rows), 0) + r * cut
        here = (tab[2:3].astype(jnp.int32) == slots) & (tab[3:4].astype(jnp.int32) == g)
        mine = jnp.where(j == 0, tab[0:1], tab[1:2])
        theirs = jnp.where(j == 0, tab[1:2], tab[0:1])
        mine = jnp.sum(jnp.where(here, mine, 0.0), axis=1, keepdims=True)
        theirs = jnp.sum(jnp.where(here, theirs, 0.0), axis=1, keepdims=True)
        es[u].wait_recv()
        value = (mine * ebuf[d, r, 0].astype(f32) + theirs * xret[d, r].astype(f32)).astype(bf16)
        if u >= 2:
            zbuf[d, r] = value
            hs[u] = send(zbuf.at[d, r], ret.at[d, r], h_s.at[d, r], h_r.at[d, r], plane(d))
        else:
            ret[0, r] = value

    def depart(u):
        d, r = units[u]
        zs[u] = send(sbuf.at[d, r], xbuf.at[0, d, r, 0], z_s.at[d, r], z_r.at[d, r], plane(d))

    sbuf[1] = gather(1).reshape(2, cut, half)
    depart(2)
    depart(3)
    own = gather(0).reshape(2, cut, half)
    for r in range(2):
        xbuf[0, 0, r, 0] = own[r]
        arrived(r)
    for d in range(2, G):
        sbuf[d] = gather(d).reshape(2, cut, half)
    for u in range(4, U):
        depart(u)
    for load in loads:
        load.wait()
    done = 2
    for u in range(U):
        while done < min(U, u + LEAD + 1):
            arrived(done)
            done += 1
        crossed(u)
        compute(u)
        summed(u)
        if u:
            mix(u - 1)
    mix(U - 1)

    eye = lax.broadcasted_iota(jnp.int32, (rows, rows), 0) == lax.broadcasted_iota(
        jnp.int32, (rows, rows), 1
    )
    back = jnp.sum(jnp.where(eye, target.astype(f32), 0.0), axis=1, keepdims=True).astype(jnp.int32)
    for copy in hs[2:]:
        copy.wait_recv()
    mixed = jnp.zeros((rows, half), f32)
    for d in range(G):
        place = lax.broadcasted_iota(jnp.int32, (rows, cap), 1) + d * cap == back
        mixed = mixed + jnp.dot(
            place.astype(f32).astype(bf16), ret[d].reshape(cap, half), preferred_element_type=f32
        )
    sq[2] = fold(mixed)
    last_sq = send(sq.at[2], sq.at[3], sq_s.at[1], sq_r.at[1], core)
    last_sq.wait_recv()
    total = jnp.sum(sq[2] + sq[3], axis=1, keepdims=True)
    norm = lax.rsqrt(total / (2 * half) + EPS)
    out_ref[...] = mixed * norm
    for copy in sent:
        copy.wait_send()


def paired(tokens, norm_gain, w_gate, w_up, w_down, expert_ids, combine, final_gain):
    rows, half = tokens.shape
    G = lax.axis_size("ep") // 2
    cap = rows // 8 * 5
    ff = w_gate.shape[2]
    vmem = pl.BlockSpec(memory_space=pltpu.VMEM)
    hbm = pl.BlockSpec(memory_space=pl.ANY)
    dma = pltpu.SemaphoreType.DMA
    out = pl.pallas_call(
        functools.partial(paired_kernel, G, cap),
        out_shape=jax.ShapeDtypeStruct((rows, half), f32),
        in_specs=[vmem] * 4 + [hbm] * 3,
        out_specs=vmem,
        scratch_shapes=[
            pltpu.VMEM((2, half, ff), bf16),
            pltpu.VMEM((2, half, ff), bf16),
            pltpu.VMEM((2, ff, half), bf16),
            pltpu.VMEM((2, G, 2, 2, cap // 2, half), bf16),
            pltpu.VMEM((G, 2, cap // 2, half), bf16),
            pltpu.VMEM((G, 8, rows), f32),
            pltpu.VMEM((G, 2, 2, cap // 2, half), bf16),
            pltpu.VMEM((G, 2, 2, cap // 2, half), bf16),
            pltpu.VMEM((G, 2, 2, cap // 2, half), bf16),
            pltpu.VMEM((G, 2, 2, cap // 2, half), bf16),
            pltpu.VMEM((G, 2, cap // 2, half), bf16),
            pltpu.VMEM((G, 2, cap // 2, half), bf16),
            pltpu.VMEM((G, 2, cap // 2, half), bf16),
            pltpu.VMEM((4, rows, 128), f32),
            dma((6,)),
            dma((2,)), dma((2,)),
            dma((G, 2)), dma((G, 2)),
            dma((G,)), dma((G,)),
            dma((G, 2)), dma((G, 2)),
            dma((G, 2, 2)), dma((G, 2, 2)),
            dma((G, 2)), dma((G, 2)),
            dma((G, 2)), dma((G, 2)),
            dma((G, 2)), dma((G, 2)),
        ],
        compiler_params=pltpu.CompilerParams(
            collective_id=0, has_side_effects=True, vmem_limit_bytes=60 * 1024 * 1024
        ),
        name="paired",
    )(
        tokens, norm_gain, expert_ids.T, combine.T, w_gate, w_up, w_down,
    )
    return (out * final_gain.astype(f32)).astype(bf16)


def body(tokens, norm_gain, w_gate, w_up, w_down, expert_ids, combine, final_gain):
    experts = w_gate.shape[0] * lax.axis_size("ep")
    per_group = experts // GROUPS
    args = (tokens, norm_gain, w_gate, w_up, w_down, expert_ids, combine, final_gain)
    if (
        per_group == expert_ids.shape[1] == 2
        and w_gate.shape[0] == 1
        and lax.axis_size("tp") == 2
        and GROUPS == 4
        and tokens.shape[0] % 256 == 0
    ):
        return paired(*args)
    return general(*args)


def solution(mesh):
    placed = (
        P(("grp", "ep"), "tp"),
        P("tp"),
        P("ep", None, "tp"),
        P("ep", None, "tp"),
        P("ep", "tp", None),
        P(("grp", "ep"), None),
        P(("grp", "ep"), None),
        P("tp"),
    )
    return jax.shard_map(
        body, mesh=mesh, in_specs=placed, out_specs=P(("grp", "ep"), "tp"), check_vma=False
    )
```

profile of v0, /device:TPU:1, one launch (start us, length us, event | category | flops | bytes accessed | tf_op | source)
XLA Modules:
  0.0 87.3 jit_solution(17139981462789306690)
XLA Ops:
  0.0 0.7 convert_element_type.6
  0.7 84.5 %paired.1 = f32[256,1024]{1,0:T(8,128)} custom-call(bf16[256,1024]{1,0:T(8,128)(2,1)} %tok_ref.1, bf16[1024]{0:T(1024)(128)(2,1)} %gain_ref.1, s32[2,256]{1,0:T(2,128)} %bitcast.2, f32[2,256]{1,0:T(2,128)} %bitcast.3, bf16[1,2048,512]{2,1,0:T(8,128)(2,1)} %wg_hbm.1, bf16[1,2048,512]{2,1,0:T(8,128)(2,1)} %wu_hbm.1, bf16[1,512,2048]{2,1,0:T(8,128)(2,1)} %wd_hbm.1), custom_call_target="tpu_custom_call" | custom-call | tf_op jit(solution)/shard_map/paired/pallas_call | solution.py:287
  85.2 2.1 %multiply_convert_fusion = bf16[256,1024]{1,0:T(8,128)(2,1)} fusion(f32[256,1024]{1,0:T(8,128)} %paired.1, f32[1024]{0:T(1024)S(1)} %convert_element_type.6), kind=kLoop, calls=%fused_computation | loop fusion | flops 524288 | bytes 1576960 | tf_op jit(solution)/shard_map/convert_element_type | solution.py:324
where the time goes:
time: 87.5 us; the launch traced here: 87.3 us
  Pallas kernels  84.5 us (97%)
  other arithmetic  2.8 us (3%)
    pallas_call x1, Pallas kernels, paired(): pl.pallas_call(functools.partial(paired_kernel, G, cap), out_shape=jax.Sh...  84.5 us
    convert_element_type x2, other arithmetic, paired(): return (out * final_gain.astype(f32)).astype(bf16)  2.8 us

commit v1 on v0

--- a/solution.py
+++ b/solution.py
@@ -9,7 +9,6 @@
 
 GROUPS = 4
 EPS = 1e-06
-LEAD = 1
 MESH = pl.DeviceIdType.MESH
 bf16, f32 = jnp.bfloat16, jnp.float32
 
@@ -80,26 +79,33 @@
 
 
 def paired_kernel(
-    G, cap, tok_ref, gain_ref, ids_ref, comb_ref, wg_hbm, wu_hbm, wd_hbm, out_ref,
-    wg, wu, wd, xbuf, sbuf, meta, psend, pown, precv, ebuf, xret, zbuf, ret, sq,
-    wsem, sq_s, sq_r, z_s, z_r, m_s, m_r, x_s, x_r, t_s, t_r, p_s, p_r, e_s, e_r, h_s, h_r,
+    G, cap, tok_hbm, gain_hbm, ids_hbm, comb_hbm, fgain_hbm, wg_hbm, wu_hbm, wd_hbm, out_ref,
+    wg, wu, wd, xbuf, sbuf, rawx, meta, psend, pown, precv, ebuf, xret, zbuf, ret, sq, acc,
+    tok_ref, gain_ref, ids_ref, comb_ref, fgain_ref,
+    fetch_s, wsem, sq_s, sq_r, z_s, z_r, m_s, m_r, x_s, x_r, t_s, t_r, p_s, p_r, e_s, e_r,
+    h_s, h_r,
 ):
-    rows, half = tok_ref.shape
+    rows, half = tok_hbm.shape
     ep, c = lax.axis_index("ep"), lax.axis_index("tp")
     g, j = ep // 2, ep % 2
     other = {"ep": g * 2 + (1 - j)}
     core = {"tp": 1 - c}
-
     cut = cap // 2
+
+    operands = (tok_hbm, gain_hbm, ids_hbm, comb_hbm, fgain_hbm)
+    staged = (tok_ref, gain_ref, ids_ref, comb_ref, fgain_ref)
+    fetches = [
+        pltpu.make_async_copy(src, dst, fetch_s.at[i])
+        for i, (src, dst) in enumerate(zip(operands, staged))
+    ]
+    for fetch in fetches:
+        fetch.start()
 
     def flip(a, d):
         return (a % 2 + d % 2) % 2 + 2 * ((a // 2 + d // 2) % 2)
 
     def plane(d):
         return {"ep": flip(g, d) * 2 + j}
-
-    inner = ((g + 1) // 2) % 2
-    order = [0, 1, 2 + inner, 3 - inner]
 
     barrier = pltpu.get_barrier_semaphore()
     for dev in [core, other] + [plane(d) for d in range(1, G)]:
@@ -111,8 +117,6 @@
         loads.append(pltpu.make_async_copy(wg_hbm.at[0, at, :], wg.at[i], wsem.at[i]))
         loads.append(pltpu.make_async_copy(wu_hbm.at[0, at, :], wu.at[i], wsem.at[2 + i]))
         loads.append(pltpu.make_async_copy(wd_hbm.at[0, :, at], wd.at[i], wsem.at[4 + i]))
-    for load in loads:
-        load.start()
 
     sent = []
 
@@ -124,9 +128,8 @@
         sent.append(copy)
         return copy
 
-    x = tok_ref[...].astype(f32)
-    sq[0] = fold(x)
-
+    fetches[2].wait()
+    fetches[3].wait()
     group = ids_ref[0:1, :] // 2
     slot8 = lax.broadcasted_iota(jnp.int32, (8, rows), 0)
     onehot = (slot8 == group).astype(f32)
@@ -143,45 +146,89 @@
     table = jnp.where(slot8 == 1, jnp.where(first, c1, c0), table)
     table = jnp.where(slot8 == 2, rank, table)
     table = jnp.where(slot8 == 3, group.astype(f32), table)
-    meta[0] = table
     pick = (lax.broadcasted_iota(jnp.int32, (G * cap, rows), 0) == target).astype(f32).astype(bf16)
+    eye = lax.broadcasted_iota(jnp.int32, (rows, rows), 0) == lax.broadcasted_iota(
+        jnp.int32, (rows, rows), 1
+    )
+
+    def gather(d):
+        return jnp.dot(
+            pick[d * cap : (d + 1) * cap], tok_ref[...], preferred_element_type=f32
+        ).astype(bf16).reshape(2, cut, half)
+
+    fetches[0].wait()
+    sbuf[0] = gather(0)
+    sbuf[1] = gather(1)
+    sbuf[3] = gather(3)
+    x = tok_ref[...].astype(f32)
+    sq[0] = fold(x)
+
+    O0, O1, N0, N1, F1, F2, F3, F4 = [
+        (0, 0), (0, 1), (1, 0), (1, 1), (3, 0), (2, 0), (3, 1), (2, 1)
+    ]
+    zs, xs, ts, fs, ps, es, hs = ({} for _ in range(7))
+
+    def depart(u):
+        d, r = u
+        zs[u] = send(sbuf.at[d, r], rawx.at[d, r], z_s.at[d, r], z_r.at[d, r], plane(d))
 
     pl.semaphore_wait(barrier, 1 + G)
+    xs[O0] = send(sbuf.at[0, 0], rawx.at[0, 0], x_s.at[0, 0], x_r.at[0, 0], other)
+    depart(N0)
     first_sq = send(sq.at[0], sq.at[1], sq_s.at[0], sq_r.at[0], core)
-    metas = [None] + [
-        send(meta.at[0], meta.at[d], m_s.at[d], m_r.at[d], plane(d)) for d in order[1:]
-    ]
+    sbuf[2] = gather(2)
     first_sq.wait_recv()
     total = jnp.sum(sq[0] + sq[1], axis=1, keepdims=True)
     scale = lax.rsqrt(total / (2 * half) + EPS)
-    normed = (x * scale * gain_ref[...].astype(f32)[None, :]).astype(bf16)
-
-    def gather(d):
-        return jnp.dot(
-            pick[d * cap : (d + 1) * cap], normed, preferred_element_type=f32
-        ).astype(bf16)
-
-    units = [(d, r) for d in order for r in range(2)]
-    U = len(units)
-    zs, xs, ts, fs, ps, es, hs = ([None] * U for _ in range(7))
-
-    def arrived(u):
-        d, r = units[u]
-        if zs[u] is not None:
+    across = jnp.sum(jnp.where(eye, scale, 0.0), axis=0, keepdims=True)
+    meta[0] = jnp.where(slot8 == 4, across, table)
+    metas = {
+        d: send(meta.at[0], meta.at[d], m_s.at[d], m_r.at[d], plane(d)) for d in (1, 3, 2)
+    }
+    metas[G] = send(meta.at[0], meta.at[G], m_s.at[G], m_r.at[G], other)
+    xs[O1] = send(sbuf.at[0, 1], rawx.at[0, 1], x_s.at[0, 1], x_r.at[0, 1], other)
+    for load in loads:
+        load.start()
+    fetches[1].wait()
+    fetches[4].wait()
+    gain = gain_ref[...].astype(f32)[None, :]
+    waited = set()
+
+    def sloted(d, r, *names):
+        if d and d not in waited:
+            waited.add(d)
+            metas[d].wait_recv()
+        tab = meta[d]
+        slots = lax.broadcasted_iota(jnp.int32, (cut, rows), 0) + r * cut
+        here = (tab[2:3].astype(jnp.int32) == slots) & (tab[3:4].astype(jnp.int32) == g)
+        return [jnp.sum(jnp.where(here, name(tab), 0.0), axis=1, keepdims=True) for name in names]
+
+    def normed(raw, d, r):
+        (by,) = sloted(d, r, lambda tab: tab[4:5])
+        return (raw.astype(f32) * by * gain).astype(bf16)
+
+    def dispatch(u):
+        d, r = u
+        mine = xbuf.at[0, d, r, 0]
+        if d:
             zs[u].wait_recv()
-        mine = xbuf.at[0, d, r, 0]
-        xs[u] = send(mine, xbuf.at[0, d, r, 1], x_s.at[d, r], x_r.at[d, r], other)
+            xbuf[0, d, r, 0] = normed(rawx[d, r], d, r)
+            xs[u] = send(mine, xbuf.at[0, d, r, 1], x_s.at[d, r], x_r.at[d, r], other)
+        else:
+            xbuf[0, d, r, 0] = normed(sbuf[0, r], 0, r)
         ts[u] = send(mine, xbuf.at[1, d, r, 0], t_s.at[d, r, 0], t_r.at[d, r, 0], core)
 
-    def crossed(u):
-        d, r = units[u]
+    def forward(u):
+        d, r = u
         xs[u].wait_recv()
+        if d == 0:
+            xbuf[0, 0, r, 1] = normed(rawx[0, r], G, r)
         fs[u] = send(
             xbuf.at[0, d, r, 1], xbuf.at[1, d, r, 1], t_s.at[d, r, 1], t_r.at[d, r, 1], core
         )
 
     def compute(u):
-        d, r = units[u]
+        d, r = u
         ts[u].wait_recv()
         fs[u].wait_recv()
         a = xbuf[0, d, r].reshape(2 * cut, half)
@@ -200,78 +247,67 @@
         pown[d, r] = home.astype(bf16).reshape(2, cut, half)
 
     def summed(u):
-        d, r = units[u]
+        d, r = u
         ps[u].wait_recv()
         ebuf[d, r, 1] = (pown[d, r, 1].astype(f32) + precv[d, r, 1].astype(f32)).astype(bf16)
         es[u] = send(ebuf.at[d, r, 1], xret.at[d, r], e_s.at[d, r], e_r.at[d, r], other)
         ebuf[d, r, 0] = (pown[d, r, 0].astype(f32) + precv[d, r, 0].astype(f32)).astype(bf16)
 
     def mix(u):
-        d, r = units[u]
-        if u >= 2 and r == 0:
-            metas[u // 2].wait_recv()
-        tab = meta[d]
-        slots = lax.broadcasted_iota(jnp.int32, (cut, rows), 0) + r * cut
-        here = (tab[2:3].astype(jnp.int32) == slots) & (tab[3:4].astype(jnp.int32) == g)
-        mine = jnp.where(j == 0, tab[0:1], tab[1:2])
-        theirs = jnp.where(j == 0, tab[1:2], tab[0:1])
-        mine = jnp.sum(jnp.where(here, mine, 0.0), axis=1, keepdims=True)
-        theirs = jnp.sum(jnp.where(here, theirs, 0.0), axis=1, keepdims=True)
+        d, r = u
+        mine, theirs = sloted(
+            d, r,
+            lambda tab: jnp.where(j == 0, tab[0:1], tab[1:2]),
+            lambda tab: jnp.where(j == 0, tab[1:2], tab[0:1]),
+        )
         es[u].wait_recv()
         value = (mine * ebuf[d, r, 0].astype(f32) + theirs * xret[d, r].astype(f32)).astype(bf16)
-        if u >= 2:
+        if d:
             zbuf[d, r] = value
             hs[u] = send(zbuf.at[d, r], ret.at[d, r], h_s.at[d, r], h_r.at[d, r], plane(d))
         else:
             ret[0, r] = value
 
-    def depart(u):
-        d, r = units[u]
-        zs[u] = send(sbuf.at[d, r], xbuf.at[0, d, r, 0], z_s.at[d, r], z_r.at[d, r], plane(d))
-
-    sbuf[1] = gather(1).reshape(2, cut, half)
-    depart(2)
-    depart(3)
-    own = gather(0).reshape(2, cut, half)
-    for r in range(2):
-        xbuf[0, 0, r, 0] = own[r]
-        arrived(r)
-    for d in range(2, G):
-        sbuf[d] = gather(d).reshape(2, cut, half)
-    for u in range(4, U):
-        depart(u)
-    for load in loads:
-        load.wait()
-    done = 2
-    for u in range(U):
-        while done < min(U, u + LEAD + 1):
-            arrived(done)
-            done += 1
-        crossed(u)
-        compute(u)
-        summed(u)
-        if u:
-            mix(u - 1)
-    mix(U - 1)
-
-    eye = lax.broadcasted_iota(jnp.int32, (rows, rows), 0) == lax.broadcasted_iota(
-        jnp.int32, (rows, rows), 1
-    )
     back = jnp.sum(jnp.where(eye, target.astype(f32), 0.0), axis=1, keepdims=True).astype(jnp.int32)
-    for copy in hs[2:]:
-        copy.wait_recv()
-    mixed = jnp.zeros((rows, half), f32)
-    for d in range(G):
-        place = lax.broadcasted_iota(jnp.int32, (rows, cap), 1) + d * cap == back
-        mixed = mixed + jnp.dot(
-            place.astype(f32).astype(bf16), ret[d].reshape(cap, half), preferred_element_type=f32
-        )
-    sq[2] = fold(mixed)
+    sums = []
+
+    def gathered(u):
+        d, r = u
+        if d:
+            hs[u].wait_recv()
+        place = lax.broadcasted_iota(jnp.int32, (rows, cut), 1) + (d * cap + r * cut) == back
+        part = jnp.dot(place.astype(f32).astype(bf16), ret[d, r], preferred_element_type=f32)
+        acc[...] = acc[...] + part if sums else part
+        sums.append(u)
+
+    def arm(u):
+        if u == O0:
+            for load in loads:
+                load.wait()
+
+    schedule = (
+        (depart, F1), (dispatch, N0), (depart, N1), (depart, F2), (dispatch, F1),
+        (dispatch, N1), (depart, F3), (forward, F1), (forward, N0), (dispatch, O0),
+        (dispatch, F2), (arm, O0), (compute, F1), (summed, F1), (forward, O0),
+        (depart, F4), (forward, F2), (dispatch, F3), (compute, F2), (compute, O0),
+        (summed, F2), (forward, N1), (mix, F1), (forward, F3), (dispatch, F4),
+        (dispatch, O1), (compute, N0), (compute, F3), (summed, F3), (summed, N0),
+        (mix, F2), (forward, O1), (compute, N1), (forward, F4), (compute, F4),
+        (summed, F4), (mix, F3), (summed, N1), (summed, O0), (mix, N0),
+        (gathered, F2), (compute, O1), (summed, O1), (gathered, F1), (mix, F4),
+        (mix, N1), (mix, O0), (gathered, O0), (gathered, N0), (gathered, F3),
+        (gathered, F4), (gathered, N1), (mix, O1), (gathered, O1),
+    )
+    for step, u in schedule:
+        step(u)
+
+    sq[2] = fold(acc[...])
     last_sq = send(sq.at[2], sq.at[3], sq_s.at[1], sq_r.at[1], core)
     last_sq.wait_recv()
     total = jnp.sum(sq[2] + sq[3], axis=1, keepdims=True)
     norm = lax.rsqrt(total / (2 * half) + EPS)
-    out_ref[...] = mixed * norm
+    fgain = fgain_ref[...].astype(f32)[None, :]
+    out_ref[...] = (acc[...] * norm * fgain).astype(bf16)
     for copy in sent:
         copy.wait_send()
 
@@ -281,33 +317,41 @@
     G = lax.axis_size("ep") // 2
     cap = rows // 8 * 5
     ff = w_gate.shape[2]
-    vmem = pl.BlockSpec(memory_space=pltpu.VMEM)
     hbm = pl.BlockSpec(memory_space=pl.ANY)
     dma = pltpu.SemaphoreType.DMA
-    out = pl.pallas_call(
+    units = (G, 2, cap // 2, half)
+    pairs = (G, 2, 2, cap // 2, half)
+    return pl.pallas_call(
         functools.partial(paired_kernel, G, cap),
-        out_shape=jax.ShapeDtypeStruct((rows, half), f32),
-        in_specs=[vmem] * 4 + [hbm] * 3,
-        out_specs=vmem,
+        out_shape=pltpu.VMEM((rows, half), bf16),
+        in_specs=[hbm] * 8,
+        out_specs=pl.BlockSpec(memory_space=pltpu.VMEM),
         scratch_shapes=[
             pltpu.VMEM((2, half, ff), bf16),
             pltpu.VMEM((2, half, ff), bf16),
             pltpu.VMEM((2, ff, half), bf16),
-            pltpu.VMEM((2, G, 2, 2, cap // 2, half), bf16),
-            pltpu.VMEM((G, 2, cap // 2, half), bf16),
-            pltpu.VMEM((G, 8, rows), f32),
-            pltpu.VMEM((G, 2, 2, cap // 2, half), bf16),
-            pltpu.VMEM((G, 2, 2, cap // 2, half), bf16),
-            pltpu.VMEM((G, 2, 2, cap // 2, half), bf16),
-            pltpu.VMEM((G, 2, 2, cap // 2, half), bf16),
-            pltpu.VMEM((G, 2, cap // 2, half), bf16),
-            pltpu.VMEM((G, 2, cap // 2, half), bf16),
-            pltpu.VMEM((G, 2, cap // 2, half), bf16),
+            pltpu.VMEM((2,) + pairs, bf16),
+            pltpu.VMEM(units, bf16),
+            pltpu.VMEM(units, bf16),
+            pltpu.VMEM((G + 1, 8, rows), f32),
+            pltpu.VMEM(pairs, bf16),
+            pltpu.VMEM(pairs, bf16),
+            pltpu.VMEM(pairs, bf16),
+            pltpu.VMEM(pairs, bf16),
+            pltpu.VMEM(units, bf16),
+            pltpu.VMEM(units, bf16),
+            pltpu.VMEM(units, bf16),
             pltpu.VMEM((4, rows, 128), f32),
-            dma((6,)),
+            pltpu.VMEM((rows, half), f32),
+            pltpu.VMEM((rows, half), bf16),
+            pltpu.VMEM((half,), bf16),
+            pltpu.VMEM((2, rows), jnp.int32),
+            pltpu.VMEM((2, rows), f32),
+            pltpu.VMEM((half,), bf16),
+            dma((5,)), dma((6,)),
             dma((2,)), dma((2,)),
             dma((G, 2)), dma((G, 2)),
-            dma((G,)), dma((G,)),
+            dma((G + 1,)), dma((G + 1,)),
             dma((G, 2)), dma((G, 2)),
             dma((G, 2, 2)), dma((G, 2, 2)),
             dma((G, 2)), dma((G, 2)),
@@ -315,13 +359,12 @@
             dma((G, 2)), dma((G, 2)),
         ],
         compiler_params=pltpu.CompilerParams(
-            collective_id=0, has_side_effects=True, vmem_limit_bytes=60 * 1024 * 1024
+            collective_id=0, has_side_effects=True, vmem_limit_bytes=57 * 1024 * 1024
         ),
         name="paired",
     )(
-        tokens, norm_gain, expert_ids.T, combine.T, w_gate, w_up, w_down,
-    )
-    return (out * final_gain.astype(f32)).astype(bf16)
+        tokens, norm_gain, expert_ids.T, combine.T, final_gain, w_gate, w_up, w_down,
+    )
 
 
 def body(tokens, norm_gain, w_gate, w_up, w_down, expert_ids, combine, final_gain):

time: 87.5 us -> 70.2 us (0.80)
  Pallas kernels: 84.5 us -> 69 us
  other arithmetic: 2.8 us -> 0 us
    pallas_call x1, Pallas kernels: 84.5 us -> 69 us  [paired(): pl.pallas_call(functools.partial(paired_kernel, G, cap), out_shape=pltpu....]
    convert_element_type x2 -> x0, other arithmetic: 2.8 us -> none  [paired(): return (out * final_gain.astype(f32)).astype(bf16)]
where the time goes in v1:
time: 70.2 us; the launch traced here: 69.8 us
  Pallas kernels  69 us (98%)
  local copies, waits for them, and re-layouts  0.8 us (1%)
    pallas_call x1, Pallas kernels, paired(): pl.pallas_call(functools.partial(paired_kernel, G, cap), out_shape=pltpu....  69 us

profile of v1, /device:TPU:1, one launch (start us, length us, event | category | flops | bytes accessed | tf_op | source)
XLA Modules:
  0.0 69.8 jit_solution(4427829399136372631)
XLA Ops:
  0.0 69.0 %paired.1 = bf16[256,1024]{1,0:T(8,128)(2,1)S(1)} custom-call(bf16[256,1024]{1,0:T(8,128)(2,1)} %tok_hbm.1, bf16[1024]{0:T(1024)(128)(2,1)} %gain_hbm.1, s32[2,256]{1,0:T(2,128)} %bitcast.2, f32[2,256]{1,0:T(2,128)} %bitcast.3, bf16[1024]{0:T(1024)(128)(2,1)} %fgain_hbm.1, bf16[1,2048,512]{2,1,0:T(8,128)(2,1)} %wg_hbm.1, bf16[1,2048,512]{2,1,0:T(8,128)(2,1)} %wu_hbm.1, ...), custom_call_target="tpu_custom_call" | custom-call | tf_op jit(solution)/shard_map/paired/pallas_call | solution.py:324
  69.0 0.8 %copy.10 = bf16[256,1024]{1,0:T(8,128)(2,1)} copy(bf16[256,1024]{1,0:T(8,128)(2,1)S(1)} %paired.1) | data formatting | bytes 1048576

commit v2 on v1

--- a/solution.py
+++ b/solution.py
@@ -108,24 +108,27 @@
         return {"ep": flip(g, d) * 2 + j}
 
     barrier = pltpu.get_barrier_semaphore()
-    for dev in [core, other] + [plane(d) for d in range(1, G)]:
+
+    def greet(dev):
         pl.semaphore_signal(barrier, inc=1, device_id=dev, device_id_type=MESH)
+
+    greet(core)
+    greet(other)
+    for d in range(1, G):
+        pl.when((g != 0) & (g != d))(functools.partial(greet, plane(d)))
 
     loads = []
     for i, h in enumerate((c, 1 - c)):
         at = pl.ds(pl.multiple_of(h * half, half), half)
-        loads.append(pltpu.make_async_copy(wg_hbm.at[0, at, :], wg.at[i], wsem.at[i]))
-        loads.append(pltpu.make_async_copy(wu_hbm.at[0, at, :], wu.at[i], wsem.at[2 + i]))
-        loads.append(pltpu.make_async_copy(wd_hbm.at[0, :, at], wd.at[i], wsem.at[4 + i]))
-
-    sent = []
+        loads.append(pltpu.make_async_copy(wg_hbm.at[0, at, :], wg.at[i], wsem.at[0]))
+        loads.append(pltpu.make_async_copy(wu_hbm.at[0, at, :], wu.at[i], wsem.at[1]))
+        loads.append(pltpu.make_async_copy(wd_hbm.at[0, :, at], wd.at[i], wsem.at[2]))
 
     def send(src, dst, s, r, dev):
         copy = pltpu.make_async_remote_copy(
             src_ref=src, dst_ref=dst, send_sem=s, recv_sem=r, device_id=dev, device_id_type=MESH
         )
         copy.start()
-        sent.append(copy)
         return copy
 
     fetches[2].wait()
@@ -151,6 +154,9 @@
         jnp.int32, (rows, rows), 1
     )
 
+    def across(column):
+        return jnp.where(slot8 == 0, jnp.sum(jnp.where(eye, column, 0.0), axis=0, keepdims=True), 0.0)
+
     def gather(d):
         return jnp.dot(
             pick[d * cap : (d + 1) * cap], tok_ref[...], preferred_element_type=f32
@@ -158,35 +164,50 @@
 
     fetches[0].wait()
     sbuf[0] = gather(0)
-    sbuf[1] = gather(1)
-    sbuf[3] = gather(3)
-    x = tok_ref[...].astype(f32)
-    sq[0] = fold(x)
-
     O0, O1, N0, N1, F1, F2, F3, F4 = [
         (0, 0), (0, 1), (1, 0), (1, 1), (3, 0), (2, 0), (3, 1), (2, 1)
     ]
     zs, xs, ts, fs, ps, es, hs = ({} for _ in range(7))
 
+    @pl.when(g == 0)
+    def _():
+        pl.semaphore_wait(barrier, 2)
+        for d in range(1, G):
+            greet(plane(d))
+
+    @pl.when(g != 0)
+    def _():
+        pl.semaphore_wait(barrier, 1 + G)
+        greet({"ep": j})
+
     def depart(u):
         d, r = u
-        zs[u] = send(sbuf.at[d, r], rawx.at[d, r], z_s.at[d, r], z_r.at[d, r], plane(d))
-
-    pl.semaphore_wait(barrier, 1 + G)
-    xs[O0] = send(sbuf.at[0, 0], rawx.at[0, 0], x_s.at[0, 0], x_r.at[0, 0], other)
-    depart(N0)
+        zs[u] = send(sbuf.at[d, r], rawx.at[d, r], z_s, z_r.at[d - 1, r], plane(d))
+
+    xs[O0] = send(sbuf.at[0, 0], rawx.at[0, 0], x_s, x_r.at[0, 0], other)
+    sbuf[1] = gather(1)
+    zs[N0] = pltpu.make_async_remote_copy(
+        src_ref=sbuf.at[1, 0], dst_ref=rawx.at[1, 0], send_sem=z_s, recv_sem=z_r.at[0, 0],
+        device_id=plane(1), device_id_type=MESH,
+    )
+    pl.when(g != 0)(zs[N0].start)
+    sq[0] = across(jnp.sum(fold(tok_ref[...].astype(f32)), axis=1, keepdims=True))
     first_sq = send(sq.at[0], sq.at[1], sq_s.at[0], sq_r.at[0], core)
+    sbuf[3] = gather(3)
     sbuf[2] = gather(2)
     first_sq.wait_recv()
-    total = jnp.sum(sq[0] + sq[1], axis=1, keepdims=True)
-    scale = lax.rsqrt(total / (2 * half) + EPS)
-    across = jnp.sum(jnp.where(eye, scale, 0.0), axis=0, keepdims=True)
-    meta[0] = jnp.where(slot8 == 4, across, table)
-    metas = {
-        d: send(meta.at[0], meta.at[d], m_s.at[d], m_r.at[d], plane(d)) for d in (1, 3, 2)
-    }
-    metas[G] = send(meta.at[0], meta.at[G], m_s.at[G], m_r.at[G], other)
-    xs[O1] = send(sbuf.at[0, 1], rawx.at[0, 1], x_s.at[0, 1], x_r.at[0, 1], other)
+    scale = lax.rsqrt((sq[0, 0:1] + sq[1, 0:1]) / (2 * half) + EPS)
+    meta[0] = jnp.where(slot8 == 4, scale, table)
+    metas = {G: send(meta.at[0], meta.at[G], m_s, m_r.at[G - 1], other)}
+    xs[O1] = send(sbuf.at[0, 1], rawx.at[0, 1], x_s, x_r.at[0, 1], other)
+
+    @pl.when(g == 0)
+    def _():
+        pl.semaphore_wait(barrier, G - 1)
+        zs[N0].start()
+
+    for d in (1, 3, 2):
+        metas[d] = send(meta.at[0], meta.at[d], m_s, m_r.at[d - 1], plane(d))
     for load in loads:
         load.start()
     fetches[1].wait()
@@ -213,10 +234,10 @@
         if d:
             zs[u].wait_recv()
             xbuf[0, d, r, 0] = normed(rawx[d, r], d, r)
-            xs[u] = send(mine, xbuf.at[0, d, r, 1], x_s.at[d, r], x_r.at[d, r], other)
+            xs[u] = send(mine, xbuf.at[0, d, r, 1], x_s, x_r.at[d, r], other)
         else:
             xbuf[0, d, r, 0] = normed(sbuf[0, r], 0, r)
-        ts[u] = send(mine, xbuf.at[1, d, r, 0], t_s.at[d, r, 0], t_r.at[d, r, 0], core)
+        ts[u] = send(mine, xbuf.at[1, d, r, 0], t_s.at[0], t_r.at[d, r], core)
 
     def forward(u):
         d, r = u
@@ -224,13 +245,13 @@
         if d == 0:
             xbuf[0, 0, r, 1] = normed(rawx[0, r], G, r)
         fs[u] = send(
-            xbuf.at[0, d, r, 1], xbuf.at[1, d, r, 1], t_s.at[d, r, 1], t_r.at[d, r, 1], core
+            xbuf.at[0, d, r, 1], xbuf.at[1, d, r, 1], t_s.at[1], t_r.at[d, r], core
         )
 
     def compute(u):
         d, r = u
-        ts[u].wait_recv()
-        fs[u].wait_recv()
+        whole = xbuf.at[1, d, r]
+        pltpu.make_async_copy(whole, whole, t_r.at[d, r]).wait()
         a = xbuf[0, d, r].reshape(2 * cut, half)
         b = xbuf[1, d, r].reshape(2 * cut, half)
         gate = jnp.dot(a, wg[0], preferred_element_type=f32) + jnp.dot(
@@ -242,7 +263,7 @@
         hidden = (gate / (1.0 + jnp.exp(-gate)) * upper).astype(bf16)
         away = jnp.dot(hidden, wd[1], preferred_element_type=f32)
         psend[d, r] = away.astype(bf16).reshape(2, cut, half)
-        ps[u] = send(psend.at[d, r], precv.at[d, r], p_s.at[d, r], p_r.at[d, r], core)
+        ps[u] = send(psend.at[d, r], precv.at[d, r], p_s, p_r.at[d, r], core)
         home = jnp.dot(hidden, wd[0], preferred_element_type=f32)
         pown[d, r] = home.astype(bf16).reshape(2, cut, half)
 
@@ -250,7 +271,7 @@
         d, r = u
         ps[u].wait_recv()
         ebuf[d, r, 1] = (pown[d, r, 1].astype(f32) + precv[d, r, 1].astype(f32)).astype(bf16)
-        es[u] = send(ebuf.at[d, r, 1], xret.at[d, r], e_s.at[d, r], e_r.at[d, r], other)
+        es[u] = send(ebuf.at[d, r, 1], xret.at[d, r], e_s, e_r.at[d, r], other)
         ebuf[d, r, 0] = (pown[d, r, 0].astype(f32) + precv[d, r, 0].astype(f32)).astype(bf16)
 
     def mix(u):
@@ -264,7 +285,7 @@
         value = (mine * ebuf[d, r, 0].astype(f32) + theirs * xret[d, r].astype(f32)).astype(bf16)
         if d:
             zbuf[d, r] = value
-            hs[u] = send(zbuf.at[d, r], ret.at[d, r], h_s.at[d, r], h_r.at[d, r], plane(d))
+            hs[u] = send(zbuf.at[d, r], ret.at[d, r], h_s, h_r.at[d - 1, r], plane(d))
         else:
             ret[0, r] = value
 
@@ -282,34 +303,39 @@
 
     def arm(u):
         if u == O0:
-            for load in loads:
-                load.wait()
+            for i, ref in enumerate((wg, wu, wd)):
+                pltpu.make_async_copy(ref, ref, wsem.at[i]).wait()
 
     schedule = (
-        (depart, F1), (dispatch, N0), (depart, N1), (depart, F2), (dispatch, F1),
-        (dispatch, N1), (depart, F3), (forward, F1), (forward, N0), (dispatch, O0),
-        (dispatch, F2), (arm, O0), (compute, F1), (summed, F1), (forward, O0),
-        (depart, F4), (forward, F2), (dispatch, F3), (compute, F2), (compute, O0),
-        (summed, F2), (forward, N1), (mix, F1), (forward, F3), (dispatch, F4),
-        (dispatch, O1), (compute, N0), (compute, F3), (summed, F3), (summed, N0),
-        (mix, F2), (forward, O1), (compute, N1), (forward, F4), (compute, F4),
-        (summed, F4), (mix, F3), (summed, N1), (summed, O0), (mix, N0),
-        (gathered, F2), (compute, O1), (summed, O1), (gathered, F1), (mix, F4),
-        (mix, N1), (mix, O0), (gathered, O0), (gathered, N0), (gathered, F3),
-        (gathered, F4), (gathered, N1), (mix, O1), (gathered, O1),
+        (dispatch, O0), (depart, F1), (depart, N1), (depart, F2), (dispatch, N0),
+        (dispatch, F1), (forward, N0), (dispatch, N1), (depart, F3), (arm, O0),
+        (compute, N0), (summed, N0), (dispatch, F2), (forward, F1), (compute, F1),
+        (depart, F4), (forward, N1), (mix, N0), (dispatch, O1), (summed, F1),
+        (dispatch, F3), (forward, F2), (compute, N1), (compute, F2), (summed, F2),
+        (mix, F1), (forward, F3), (dispatch, F4), (compute, F3), (summed, F3),
+        (forward, O0), (summed, N1), (mix, F2), (forward, F4), (compute, F4),
+        (forward, O1), (mix, F3), (summed, F4), (compute, O1), (summed, O1),
+        (gathered, F2), (mix, N1), (compute, O0), (gathered, N0), (summed, O0),
+        (gathered, F1), (mix, F4), (gathered, F3), (mix, O1), (gathered, O1),
+        (gathered, N1), (mix, O0), (gathered, O0), (gathered, F4),
     )
     for step, u in schedule:
         step(u)
 
-    sq[2] = fold(acc[...])
+    sq[2] = across(jnp.sum(fold(acc[...]), axis=1, keepdims=True))
     last_sq = send(sq.at[2], sq.at[3], sq_s.at[1], sq_r.at[1], core)
     last_sq.wait_recv()
-    total = jnp.sum(sq[2] + sq[3], axis=1, keepdims=True)
-    norm = lax.rsqrt(total / (2 * half) + EPS)
+    norm = lax.rsqrt((sq[2, 0:1] + sq[3, 0:1]) / (2 * half) + EPS)
+    norm = jnp.sum(jnp.where(eye, norm, 0.0), axis=1, keepdims=True)
     fgain = fgain_ref[...].astype(f32)[None, :]
     out_ref[...] = (acc[...] * norm * fgain).astype(bf16)
-    for copy in sent:
-        copy.wait_send()
+    drains = [
+        (sbuf.at[1:G], z_s), (meta.at[1 : G + 1], m_s), (sbuf, x_s), (sbuf, t_s.at[0]),
+        (sbuf, t_s.at[1]), (psend, p_s), (sbuf, e_s), (zbuf.at[1:G], h_s),
+        (sq.at[0], sq_s.at[0]), (sq.at[2], sq_s.at[1]),
+    ]
+    for ref, sem in drains:
+        pltpu.make_async_copy(ref, ref, sem).wait()
 
 
 def paired(tokens, norm_gain, w_gate, w_up, w_down, expert_ids, combine, final_gain):
@@ -341,22 +367,22 @@
             pltpu.VMEM(units, bf16),
             pltpu.VMEM(units, bf16),
             pltpu.VMEM(units, bf16),
-            pltpu.VMEM((4, rows, 128), f32),
+            pltpu.VMEM((4, 8, rows), f32),
             pltpu.VMEM((rows, half), f32),
             pltpu.VMEM((rows, half), bf16),
             pltpu.VMEM((half,), bf16),
             pltpu.VMEM((2, rows), jnp.int32),
             pltpu.VMEM((2, rows), f32),
             pltpu.VMEM((half,), bf16),
-            dma((5,)), dma((6,)),
+            dma((5,)), dma((3,)),
             dma((2,)), dma((2,)),
-            dma((G, 2)), dma((G, 2)),
-            dma((G + 1,)), dma((G + 1,)),
-            dma((G, 2)), dma((G, 2)),
-            dma((G, 2, 2)), dma((G, 2, 2)),
-            dma((G, 2)), dma((G, 2)),
-            dma((G, 2)), dma((G, 2)),
-            dma((G, 2)), dma((G, 2)),
+            dma, dma((G - 1, 2)),
+            dma, dma((G,)),
+            dma, dma((G, 2)),
+            dma((2,)), dma((G, 2)),
+            dma, dma((G, 2)),
+            dma, dma((G, 2)),
+            dma, dma((G - 1, 2)),
         ],
         compiler_params=pltpu.CompilerParams(
             collective_id=0, has_side_effects=True, vmem_limit_bytes=57 * 1024 * 1024

time: 70.2 us -> 68.2 us (0.972)
  Pallas kernels: 69 us -> 66.4 us
    pallas_call x1, Pallas kernels: 69 us -> 66.4 us  [paired(): pl.pallas_call(functools.partial(paired_kernel, G, cap), out_shape=pltpu....]
where the time goes in v2:
time: 68.2 us; the launch traced here: 67.2 us
  Pallas kernels  66.4 us (97%)
  local copies, waits for them, and re-layouts  0.8 us (1%)
    pallas_call x1, Pallas kernels, paired(): pl.pallas_call(functools.partial(paired_kernel, G, cap), out_shape=pltpu....  66.4 us

profile of v2, /device:TPU:1, one launch (start us, length us, event | category | flops | bytes accessed | tf_op | source)
XLA Modules:
  0.0 67.2 jit_solution(3964423120017691401)
XLA Ops:
  0.0 66.4 %paired.1 = bf16[256,1024]{1,0:T(8,128)(2,1)S(1)} custom-call(bf16[256,1024]{1,0:T(8,128)(2,1)} %tok_hbm.1, bf16[1024]{0:T(1024)(128)(2,1)} %gain_hbm.1, s32[2,256]{1,0:T(2,128)} %bitcast.2, f32[2,256]{1,0:T(2,128)} %bitcast.3, bf16[1024]{0:T(1024)(128)(2,1)} %fgain_hbm.1, bf16[1,2048,512]{2,1,0:T(8,128)(2,1)} %wg_hbm.1, bf16[1,2048,512]{2,1,0:T(8,128)(2,1)} %wu_hbm.1, ...), custom_call_target="tpu_custom_call" | custom-call | tf_op jit(solution)/shard_map/paired/pallas_call | solution.py:350
  66.4 0.8 %copy.10 = bf16[256,1024]{1,0:T(8,128)(2,1)} copy(bf16[256,1024]{1,0:T(8,128)(2,1)S(1)} %paired.1) | data formatting | bytes 1048576

commit v3 on v2

--- a/solution.py
+++ b/solution.py
@@ -292,11 +292,21 @@
     back = jnp.sum(jnp.where(eye, target.astype(f32), 0.0), axis=1, keepdims=True).astype(jnp.int32)
     sums = []
 
+    squares = []
+    last_sq = []
+
     def gathered(u):
         d, r = u
         if d:
             hs[u].wait_recv()
-        place = lax.broadcasted_iota(jnp.int32, (rows, cut), 1) + (d * cap + r * cut) == back
+        start = d * cap + r * cut
+        held = jnp.sum(fold(ret[d, r].astype(f32)), axis=1, keepdims=True)
+        at = lax.broadcasted_iota(jnp.int32, (cut, rows), 0) + start == target
+        squares.append(jnp.sum(jnp.where(at, held, 0.0), axis=0, keepdims=True))
+        if len(squares) == 2 * G:
+            sq[2] = jnp.where(slot8 == 0, sum(squares[1:], squares[0]), 0.0)
+            last_sq.append(send(sq.at[2], sq.at[3], sq_s.at[1], sq_r.at[1], core))
+        place = lax.broadcasted_iota(jnp.int32, (rows, cut), 1) + start == back
         part = jnp.dot(place.astype(f32).astype(bf16), ret[d, r], preferred_element_type=f32)
         acc[...] = acc[...] + part if sums else part
         sums.append(u)
@@ -307,24 +317,22 @@
                 pltpu.make_async_copy(ref, ref, wsem.at[i]).wait()
 
     schedule = (
-        (dispatch, O0), (depart, F1), (depart, N1), (depart, F2), (dispatch, N0),
+        (depart, F1), (dispatch, O0), (depart, N1), (dispatch, N0), (depart, F2),
         (dispatch, F1), (forward, N0), (dispatch, N1), (depart, F3), (arm, O0),
         (compute, N0), (summed, N0), (dispatch, F2), (forward, F1), (compute, F1),
-        (depart, F4), (forward, N1), (mix, N0), (dispatch, O1), (summed, F1),
-        (dispatch, F3), (forward, F2), (compute, N1), (compute, F2), (summed, F2),
-        (mix, F1), (forward, F3), (dispatch, F4), (compute, F3), (summed, F3),
-        (forward, O0), (summed, N1), (mix, F2), (forward, F4), (compute, F4),
-        (forward, O1), (mix, F3), (summed, F4), (compute, O1), (summed, O1),
-        (gathered, F2), (mix, N1), (compute, O0), (gathered, N0), (summed, O0),
-        (gathered, F1), (mix, F4), (gathered, F3), (mix, O1), (gathered, O1),
-        (gathered, N1), (mix, O0), (gathered, O0), (gathered, F4),
+        (dispatch, O1), (depart, F4), (summed, F1), (forward, N1), (dispatch, F3),
+        (mix, N0), (forward, F2), (compute, F2), (summed, F2), (mix, F1),
+        (dispatch, F4), (forward, F3), (compute, F3), (gathered, N0), (forward, O0),
+        (compute, N1), (summed, F3), (mix, F2), (summed, N1), (forward, F4),
+        (compute, O0), (compute, F4), (mix, F3), (summed, F4), (gathered, F2),
+        (mix, N1), (summed, O0), (forward, O1), (gathered, F1), (compute, O1),
+        (mix, F4), (summed, O1), (mix, O0), (gathered, O0), (gathered, F3),
+        (gathered, N1), (mix, O1), (gathered, O1), (gathered, F4),
     )
     for step, u in schedule:
         step(u)
 
-    sq[2] = across(jnp.sum(fold(acc[...]), axis=1, keepdims=True))
-    last_sq = send(sq.at[2], sq.at[3], sq_s.at[1], sq_r.at[1], core)
-    last_sq.wait_recv()
+    last_sq[0].wait_recv()
     norm = lax.rsqrt((sq[2, 0:1] + sq[3, 0:1]) / (2 * half) + EPS)
     norm = jnp.sum(jnp.where(eye, norm, 0.0), axis=1, keepdims=True)
     fgain = fgain_ref[...].astype(f32)[None, :]

time: 68.2 us -> 67.4 us (0.988); the launches traced: 67.2 us -> 67.2 us
  no operation moved by 1% of the time
where the time goes in v3:
time: 67.4 us; the launch traced here: 67.2 us
  Pallas kernels  66.4 us (99%)
  local copies, waits for them, and re-layouts  0.8 us (1%)
    pallas_call x1, Pallas kernels, paired(): pl.pallas_call(functools.partial(paired_kernel, G, cap), out_shape=pltpu....  66.4 us

profile of v3, /device:TPU:1, one launch (start us, length us, event | category | flops | bytes accessed | tf_op | source)
XLA Modules:
  0.0 67.2 jit_solution(8811924611953832839)
XLA Ops:
  0.0 66.4 %paired.1 = bf16[256,1024]{1,0:T(8,128)(2,1)S(1)} custom-call(bf16[256,1024]{1,0:T(8,128)(2,1)} %tok_hbm.1, bf16[1024]{0:T(1024)(128)(2,1)} %gain_hbm.1, s32[2,256]{1,0:T(2,128)} %bitcast.2, f32[2,256]{1,0:T(2,128)} %bitcast.3, bf16[1024]{0:T(1024)(128)(2,1)} %fgain_hbm.1, bf16[1,2048,512]{2,1,0:T(8,128)(2,1)} %wg_hbm.1, bf16[1,2048,512]{2,1,0:T(8,128)(2,1)} %wu_hbm.1, ...), custom_call_target="tpu_custom_call" | custom-call | tf_op jit(solution)/shard_map/paired/pallas_call | solution.py:358
  66.4 0.8 %copy.10 = bf16[256,1024]{1,0:T(8,128)(2,1)} copy(bf16[256,1024]{1,0:T(8,128)(2,1)S(1)} %paired.1) | data formatting | bytes 1048576
